TPU v7x, 32 devices: a whole 2x2x4 slice. The times are simulated.
32 devices in a mesh: sp: 4 (over y, x), tp: 8 (over z, core).
Axes of the slice: x: 2, y: 2, z: 4, core: 2. Of those that a mesh axis runs over, the one named last changes fastest.
Arguments:
- queries: bfloat16 [1536, 2048], P('sp', 'tp'), may hold values from -6 to 6
- keys: bfloat16 [1536, 2048], P('sp', 'tp'), may hold values from -6 to 6
- values: bfloat16 [1536, 2048], P('sp', 'tp'), may hold values from -6 to 6
- key_bias: bfloat16 [1536, 32], P('sp', 'tp'), may hold values from -16 to 0
- head_gain: float32 [32, 64], P('tp'), may hold values from 0.1 to 1.9
- out_weight: bfloat16 [2048, 2048], P('tp'), may hold values from -0.125 to 0.125
- residual: bfloat16 [1536, 2048], P(('sp', 'tp')), may hold values from -6 to 6
- norm_gain: float32 [2048], replicated, may hold values from 0.1 to 1.9
- gate_proj: bfloat16 [4, 2048, 7168], P('sp', None, 'tp'), may hold values from -0.125 to 0.125
- up_proj: bfloat16 [4, 2048, 7168], P('sp', None, 'tp'), may hold values from -0.125 to 0.125
- down_proj: bfloat16 [4, 7168, 2048], P('sp', 'tp'), may hold values from -0.0625 to 0.0625
- expert_choice: int32 [1536, 2], P(('sp', 'tp')), may hold values from 0 to 3, all different within a row; in each aligned block of 48 rows (0 to 47, 48 to 95, ...) at most 48 rows name the same one
- expert_weights: float32 [1536, 2], P(('sp', 'tp')), may hold values from 0.2 to 1
Outputs:
- layer_out: bfloat16 [1536, 2048], P(('sp', 'tp'))
Inputs may be any that keep to these rules, and one draw needn't show every extreme that they name: `expert_choice`: in each aligned block of 48 rows (the rows of one device), no expert is named more than 48 times; the two experts of a row differ.
All inputs are finite; a program needn't handle non-finite values.
Results may differ from a plain program's by a relative error of at most 0.019.
Values may be sent and summed in bfloat16 or wider, within the bound.
A program may use at most 128 MiB of HBM per device.

v0:
```python
import jax
import jax.numpy as jnp
from jax import lax
from jax.sharding import PartitionSpec as P

epsilon = 1e-06


def rms_scaled(values_in):
    return values_in * lax.rsqrt(jnp.mean(values_in * values_in, axis=-1, keepdims=True) + epsilon)


def expert_partial(row_block, gate_matrix, up_matrix, down_matrix):
    gate_part = jnp.dot(row_block, gate_matrix, preferred_element_type=jnp.float32)
    up_part = jnp.dot(row_block, up_matrix, preferred_element_type=jnp.float32)
    hidden = (jax.nn.silu(gate_part) * up_part).astype(jnp.bfloat16)
    return jnp.dot(hidden, down_matrix, preferred_element_type=jnp.float32)


def choice_ranks(routes, experts_all):
    flat_routes = routes.reshape(routes.shape[:-2] + (-1,))
    onehot = (flat_routes[..., None] == jnp.arange(experts_all, dtype=jnp.int32)).astype(jnp.int32)
    before = jnp.cumsum(onehot, axis=-2) - onehot
    return jnp.sum(before * onehot, axis=-1).reshape(routes.shape)


def slot_tokens(slot_index, targets, missing):
    flat_slots = slot_index.reshape(-1)
    owners = jnp.arange(flat_slots.shape[0], dtype=jnp.int32) // 2
    matches = flat_slots[None, :] == jnp.arange(targets, dtype=jnp.int32)[:, None]
    owner_found = jnp.sum(jnp.where(matches, owners[None, :], 0), axis=1)
    return jnp.where(jnp.any(matches, axis=1), owner_found, missing)


def on_device(
    queries,
    keys,
    values,
    key_bias,
    head_gain,
    out_weight,
    residual,
    norm_gain,
    gate_proj,
    up_proj,
    down_proj,
    expert_choice,
    expert_weights,
):
    rows_own = queries.shape[0]
    heads_here = head_gain.shape[0]
    head_size = head_gain.shape[1]
    model_width = out_weight.shape[1]
    seq_devices = lax.axis_size("sp")
    head_devices = lax.axis_size("tp")
    own_start = lax.axis_index("sp") * rows_own
    query_pos = own_start + jnp.arange(rows_own, dtype=jnp.int32)
    query_heads = queries.reshape(rows_own, heads_here, head_size)

    def key_block(slot_state, key_rows, value_rows, bias_rows, key_start):
        key_heads = key_rows.reshape(rows_own, heads_here, head_size)
        value_heads = value_rows.reshape(rows_own, heads_here, head_size)
        scores = jnp.einsum(
            "qhd,khd->hqk", query_heads, key_heads, preferred_element_type=jnp.float32
        ) * head_size ** (-0.5)
        scores = scores + bias_rows.astype(jnp.float32).T[:, None, :]
        key_pos = key_start + jnp.arange(rows_own, dtype=jnp.int32)
        earlier = (key_pos[None, :] < query_pos[:, None])[None, :, :]
        log_drops = jnp.where(earlier, jax.nn.log_sigmoid(-scores), 0.0)
        suffix = lax.cumsum(log_drops, axis=2, reverse=True) - log_drops
        within = jnp.where(earlier, jnp.exp(jax.nn.log_sigmoid(scores) + suffix), 0.0).astype(
            jnp.bfloat16
        )
        block_part = jnp.einsum(
            "hqk,khd->qhd", within, value_heads, preferred_element_type=jnp.float32
        )
        block_index = key_start // rows_own
        sums_new = lax.dynamic_update_index_in_dim(
            slot_state[0], block_part.reshape(rows_own, heads_here * head_size), block_index, 0
        )
        totals_new = lax.dynamic_update_index_in_dim(
            slot_state[1], jnp.sum(log_drops, axis=2), block_index, 0
        )
        return (sums_new, totals_new)

    empty_state = (
        jnp.zeros((seq_devices, rows_own, heads_here * head_size), jnp.float32),
        jnp.zeros((seq_devices, heads_here, rows_own), jnp.float32),
    )
    key_piece = lax.all_gather(keys, "sp", axis=0, tiled=True)
    value_piece = lax.all_gather(values, "sp", axis=0, tiled=True)
    bias_piece = lax.all_gather(key_bias, "sp", axis=0, tiled=True)

    def visit(block_count, state_in):
        offset = block_count * rows_own

        def take_rows(array):
            return lax.dynamic_slice_in_dim(array, offset, rows_own, 0)

        def compute(state_now):
            return key_block(
                state_now,
                take_rows(key_piece),
                take_rows(value_piece),
                take_rows(bias_piece),
                offset,
            )

        def keep(state_now):
            return state_now

        return lax.cond(offset <= own_start, compute, keep, state_in)

    block_sums, totals = lax.fori_loop(0, key_piece.shape[0] // rows_own, visit, empty_state)
    carried = jnp.sum(totals, axis=0, keepdims=True) - jnp.cumsum(totals, axis=0)
    factors = jnp.exp(carried).transpose(0, 2, 1)[..., None]
    mixture = jnp.sum(
        factors * block_sums.reshape(seq_devices, rows_own, heads_here, head_size), axis=0
    )
    attended = (
        (rms_scaled(mixture) * head_gain)
        .astype(jnp.bfloat16)
        .reshape(rows_own, heads_here * head_size)
    )
    row_share = rows_own // head_devices
    merged = lax.all_to_all(attended, "tp", split_axis=0, concat_axis=1, tiled=True)
    projected = jnp.dot(
        merged,
        lax.all_gather(out_weight, "tp", axis=0, tiled=True),
        preferred_element_type=jnp.float32,
    )
    stream = (residual.astype(jnp.float32) + projected).astype(jnp.bfloat16)
    normed = (rms_scaled(stream.astype(jnp.float32)) * norm_gain).astype(jnp.bfloat16)
    local_experts = gate_proj.shape[0]
    experts_all = local_experts * seq_devices
    capacity = 4 * rows_own // (head_devices * experts_all)
    own_slots = expert_choice * capacity + choice_ranks(expert_choice, experts_all)
    wanted = slot_tokens(own_slots, experts_all * capacity, row_share)
    outgoing = jnp.take(normed, wanted, axis=0, mode="fill", fill_value=0)
    arrived = lax.all_to_all(
        outgoing.reshape(seq_devices, local_experts, capacity, model_width),
        "sp",
        split_axis=0,
        concat_axis=0,
        tiled=True,
    )
    row_piece = lax.all_gather(arrived, "tp", axis=0, tiled=True)
    count_rows = row_piece.shape[0]
    partials = jnp.stack(
        [
            expert_partial(
                row_piece[:, 0].reshape(-1, model_width), gate_proj[0], up_proj[0], down_proj[0]
            ).reshape(count_rows, capacity, model_width)
        ],
        axis=1,
    )
    summed = lax.psum_scatter(partials.astype(jnp.bfloat16), "tp", scatter_dimension=0, tiled=True)
    returned = lax.all_to_all(summed, "sp", split_axis=0, concat_axis=0, tiled=True).reshape(
        experts_all * capacity, model_width
    )
    picked = jnp.take(returned, own_slots, axis=0).astype(jnp.float32)
    combined = jnp.sum(expert_weights[:, :, None] * picked, axis=1)
    return (stream.astype(jnp.float32) + combined).astype(jnp.bfloat16)


def solution(mesh):
    placed = (
        P("sp", "tp"),
        P("sp", "tp"),
        P("sp", "tp"),
        P("sp", "tp"),
        P("tp", None),
        P("tp", None),
        P(("sp", "tp"), None),
        P(),
        P("sp", None, "tp"),
        P("sp", None, "tp"),
        P("sp", "tp", None),
        P(("sp", "tp"), None),
        P(("sp", "tp"), None),
    )
    return jax.shard_map(
        on_device, mesh=mesh, in_specs=placed, out_specs=P(("sp", "tp"), None), check_vma=False
    )
```

profile of v0, /device:TPU:0, one launch (start us, length us, event | category | flops | bytes accessed | tf_op | source)
XLA Modules:
  0.0 380.5 jit_solution(13210839301603181166)
XLA Ops:
  7.3 1.1 copy.81
  8.4 1.1 copy.82
  9.4 1.7 copy.83
  11.2 11.0 %all_gather.17 = bf16[1536,4]{0,1:T(4,128)(2,1)} all-gather(bf16[384,4]{0,1:T(4,128)(2,1)} %param.20), channel_id=1, replica_groups=mesh['sp'=4,'tp'=8] {'sp'}, dimensions={0}, use_global_device_ids=true | all-gather | bytes 15360 | tf_op jit(solution)/shard_map/all_gather | solution.py:92
  22.2 12.4 %all_gather.15 = bf16[1536,256]{0,1:T(8,128)(2,1)} all-gather(bf16[384,256]{0,1:T(8,128)(2,1)S(1)} %copy.81), channel_id=1, replica_groups=mesh['sp'=4,'tp'=8] {'sp'}, dimensions={0}, use_global_device_ids=true | all-gather | bytes 983040 | tf_op jit(solution)/shard_map/all_gather | solution.py:91
  34.5 13.4 %all_gather.16 = bf16[1536,256]{0,1:T(8,128)(2,1)} all-gather(bf16[384,256]{0,1:T(8,128)(2,1)S(1)} %copy.82), channel_id=1, replica_groups=mesh['sp'=4,'tp'=8] {'sp'}, dimensions={0}, use_global_device_ids=true | all-gather | bytes 983040 | tf_op jit(solution)/shard_map/all_gather | solution.py:90
  47.9 1.3 broadcast_in_dim.84
  49.8 28.2 %while.17 = (s32[]{:T(128)}, f32[4,384,256]{1,2,0:T(8,128)}, f32[4,4,384]{2,1,0:T(4,128)}, s32[]{:T(128)}, bf16[1536,256]{0,1:T(8,128)(2,1)}, /*index=5*/bf16[15...) while((s32[]{:T(128)}, f32[4,384,256]{1,2,0:T(8,128)}, ...), condition=%wide.region_6.7_spmd.clone.clone, body=%wide.region_0.6_spmd.clone.clone.sunk | while | flops 246117120 | bytes 38572464 | solution.py:114
  49.8 28.0 %conditional.4 = ((f32[4,384,256]{1,2,0:T(8,128)}, f32[4,4,384]{2,1,0:T(4,128)})) conditional(s32[]{:T(128)} %convert_element_type.76, (f32[4,384,256]{1,2,0:T(8,128)}, f32[4,4,384]{2,1,0:T(4,128)}) %tuple.53, (s32[]{:T(128)}, bf16[1536,256]{0,1:T(8,128)(2,1)}, s32[]{:T(128)}, bf16[1536,256]{0,1:T(8,128)(2,1)}, bf16[384,4,64]{0,2,1:T(8,128)(2,1)}, ...), branch_computations={%region_1.0_spmd, %region_2.5_spmd} | conditional | flops 246117120 | bytes 38570716 | solution.py:112
  49.8 1.1 constant_dynamic-slice_fusion
  51.7 4.3 %fusion.15 = (f32[4,384]{1,0:T(4,128)S(1)}, f32[4,384,384]{1,2,0:T(8,128)S(1)}, f32[4,384,384]{2,1,0:T(8,128)}) fusion(f32[4,384]{1,0:T(4,128)S(1)} %convert_bitcast_fusion, pred[384,384]{0,1:T(8,128)(4,1)S(1)} %broadcast_compare_fusion, bf16[384,4,64]{0,2,1:T(8,128)(2,1)S(1)} %bitcast.92, bf16[384,4,64]{0,2,1:T(8,128)(2,1)} %get-tuple-element.177), kind=kOutput, calls=%fused_computation.33 | convolution fusion | flops 81984000 | bytes 5271552 | tf_op jit(solution)/shard_map/while/body/eval_jaxpr/cond/branch_1_fun/qhd,khd->hqk/dot_general | solution.py:63
  56.0 14.0 %fusion.2 = f32[4,384,3,128]{1,2,3,0:T(4,128)S(1)} fusion(f32[4,384,3,128]{1,3,2,0:T(8,128)S(1)} %bitcast.88), kind=kOutput, calls=%fused_computation.5 | output fusion | flops 74907648 | bytes 4718592 | tf_op jit(solution)/shard_map/reduce-window
  70.9 1.5 copy-done
  72.3 3.6 fusion.8
  76.3 0.8 constant_dynamic-update-slice_fusion
  78.0 0.8 reduce_sum.74
  78.7 0.8 fusion.24
  79.5 1.6 fusion.22
  83.2 4.8 %all-to-all-start = ((bf16[8,48,256]{2,1,0:T(8,128)(2,1)}), bf16[8,48,256]{2,1,0:T(8,128)(2,1)S(1)}, u32[]{:S(2)}, u32[]{:S(2)}) async-start(bf16[8,48,256]{2,1,0:T(8,128)(2,1)} %multiply_convert_fusion.2), calls=%async_computation | async-start | bytes 393216 | tf_op jit(solution)/shard_map/all_to_all | solution.py:126
  89.5 6.8 %all-to-all-done = bf16[8,48,256]{2,1,0:T(8,128)(2,1)S(1)} async-done(((bf16[8,48,256]{2,1,0:T(8,128)(2,1)}), bf16[8,48,256]{2,1,0:T(8,128)(2,1)S(1)}, u32[]{:S(2)}, u32[]{:S(2)}) %all-to-all-start) | async-done | bytes 196640 | tf_op jit(solution)/shard_map/all_to_all | solution.py:126
  96.4 5.1 %multiply_reduce_fusion.1 = (f32[48]{0:T(128)S(1)}, f32[48,2048]{1,0:T(8,128)S(1)}) fusion(bf16[48,2048]{1,0:T(8,128)(2,1)S(1)} %bitcast.94, bf16[2048,2048]{1,0:T(8,128)(2,1)} %all-gather.3.cloned.1.call-done, bf16[48,2048]{1,0:T(8,128)(2,1)S(1)} %copy-done.1), kind=kOutput, calls=%fused_computation.54 | convolution fusion | flops 403242944 | bytes 9175232 | tf_op jit(solution)/shard_map/dot_general | solution.py:127
  101.6 1.1 gather_fusion
  102.9 96.4 %all_to_all.26 = bf16[4,1,48,2048]{3,2,1,0:T(8,128)(2,1)} all-to-all(bf16[4,1,48,2048]{3,2,1,0:T(8,128)(2,1)S(1)} %broadcast_select_fusion), channel_id=1, replica_groups=mesh['sp'=4,'tp'=8] {'sp'}, dimensions={0} | all-to-all | bytes 1572864 | tf_op jit(solution)/shard_map/all_to_all | solution.py:140
  199.4 63.5 %all-gather.5.cloned.1.call-done = bf16[32,1,48,2048]{3,2,1,0:T(8,128)(2,1)} async-done(((bf16[4,1,48,2048]{3,2,1,0:T(8,128)(2,1)}), bf16[32,1,48,2048]{3,2,1,0:T(8,128)(2,1)}) %all-gather.5.cloned.1.call-update) | async-done | bytes 6291472 | tf_op jit(solution)/shard_map/all_gather | solution.py:147
  262.9 10.0 %fusion.18 = f32[1536,896]{1,0:T(8,128)S(1)} fusion(bf16[1536,2048]{1,0:T(8,128)(2,1)} %bitcast.101, bf16[1,2048,896]{2,1,0:T(8,128)(2,1)} %param.25), kind=kOutput, calls=%fused_computation.38 | convolution fusion | flops 5637144576 | bytes 15466496 | tf_op jit(solution)/shard_map/dot_general | solution.py:14
  272.9 7.1 %multiply_convert_fusion = bf16[1536,896]{1,0:T(8,128)(2,1)S(1)} fusion(f32[1536,896]{1,0:T(8,128)S(1)} %fusion.18, bf16[1536,2048]{1,0:T(8,128)(2,1)S(1)} %bitcast.102, bf16[1,2048,896]{2,1,0:T(8,128)(2,1)S(1)} %copy-done.7), kind=kOutput, calls=%fused_computation.35 | convolution fusion | flops 5645402112 | bytes 18219008 | tf_op jit(solution)/shard_map/dot_general | solution.py:15
  280.0 8.7 %convert_bitcast_fusion.1 = bf16[32,1,48,2048]{3,2,0,1:T(8,128)(2,1)} fusion(bf16[32,48,896]{2,1,0:T(8,128)(2,1)S(1)} %bitcast.103, bf16[1,896,2048]{2,1,0:T(8,128)(2,1)S(1)} %copy-done.8), kind=kOutput, calls=%fused_computation.34 | convolution fusion | flops 5640290304 | bytes 12713984 | tf_op jit(solution)/shard_map/dot_general | solution.py:17
  288.8 68.5 %reduce-scatter.2.cloned.1.call-done = bf16[4,1,48,2048]{3,2,0,1:T(8,128)(2,1)} async-done(((bf16[32,1,48,2048]{3,2,0,1:T(8,128)(2,1)}), bf16[4,1,48,2048]{3,2,0,1:T(8,128)(2,1)}) %reduce-scatter.2.cloned.1.call-update) | async-done | bytes 786448 | tf_op jit(solution)/shard_map/reduce_scatter | solution.py:157
  357.3 3.7 all-to-all-start.2
  361.5 8.6 %all-to-all-done.2 = bf16[4,1,48,2048]{3,2,1,0:T(8,128)(2,1)S(1)} async-done(((bf16[4,1,48,2048]{3,2,1,0:T(8,128)(2,1)}), bf16[4,1,48,2048]{3,2,1,0:T(8,128)(2,1)S(1)}, u32[]{:S(2)}, u32[]{:S(2)}) %all-to-all-start.2) | async-done | bytes 786464 | tf_op jit(solution)/shard_map/all_to_all | solution.py:158
  370.1 0.8 gather_fusion.1
  371.2 2.1 multiply_reduce_fusion
  (80 shorter events, 9.3 us)
Async XLA Ops:
  6.5 89.9 %all-gather.3.cloned.1.call-start = ((), (), s32[]{:S(2)}) async-start(), calls=%async_computation.4 | async-start | bytes 9437184 | tf_op jit(solution)/shard_map/all_gather | solution.py:129
  70.6 1.7 copy-start
  79.5 2.9 copy-start.4
  81.1 7.0 %copy-start.3 = (s32[48,2]{0,1:T(2,128)S(1)}, s32[48,2]{0,1:T(2,128)}, u32[]{:S(2)}) copy-start(s32[48,2]{0,1:T(2,128)} %param.28) | copy-start | bytes 1156
  81.3 15.1 %copy-start.1 = (bf16[48,2048]{1,0:T(8,128)(2,1)S(1)}, bf16[48,2048]{1,0:T(8,128)(2,1)}, u32[]{:S(2)}) copy-start(bf16[48,2048]{1,0:T(8,128)(2,1)} %param.23) | copy-start | bytes 589828
  83.2 13.1 %all-to-all-start = ((bf16[8,48,256]{2,1,0:T(8,128)(2,1)}), bf16[8,48,256]{2,1,0:T(8,128)(2,1)S(1)}, u32[]{:S(2)}, u32[]{:S(2)}) async-start(bf16[8,48,256]{2,1,0:T(8,128)(2,1)} %multiply_convert_fusion.2), calls=%async_computation | async-start | bytes 393216 | tf_op jit(solution)/shard_map/all_to_all | solution.py:126
  88.0 174.9 %all-gather.5.cloned.1.call-start = ((), (), s32[]{:S(2)}) async-start(), calls=%async_computation.5 | async-start | bytes 7077888 | tf_op jit(solution)/shard_map/all_gather | solution.py:147
  96.4 5.1 %copy-start.2 = (f32[2048]{0:T(1024)S(1)}, f32[2048]{0:T(1024)}, u32[]{:S(2)}) copy-start(f32[2048]{0:T(1024)} %param.24) | copy-start | bytes 24580
  199.3 158.0 %reduce-scatter.2.cloned.1.call-start = ((), (), s32[]{:S(2)}) async-start(), calls=%async_computation.6 | async-start | bytes 7077888 | tf_op jit(solution)/shard_map/reduce_scatter | solution.py:157
  262.9 10.0 %copy-start.6 = (bf16[32,1,48,2048]{3,2,1,0:T(8,128)(2,1)S(1)}, bf16[32,1,48,2048]{3,2,1,0:T(8,128)(2,1)}, u32[]{:S(2)}) copy-start(bf16[32,1,48,2048]{3,2,1,0:T(8,128)(2,1)} %all-gather.5.cloned.1.call-done) | copy-start | bytes 18874372
  262.9 10.0 %copy-start.7 = (bf16[1,2048,896]{2,1,0:T(8,128)(2,1)S(1)}, bf16[1,2048,896]{2,1,0:T(8,128)(2,1)}, u32[]{:S(2)}) copy-start(bf16[1,2048,896]{2,1,0:T(8,128)(2,1)} %param.26) | copy-start | bytes 11010052
  272.9 7.1 %copy-start.8 = (bf16[1,896,2048]{2,1,0:T(8,128)(2,1)S(1)}, bf16[1,896,2048]{2,1,0:T(8,128)(2,1)}, u32[]{:S(2)}) copy-start(bf16[1,896,2048]{2,1,0:T(8,128)(2,1)} %param.27) | copy-start | bytes 11010052
  288.8 72.6 %copy-start.5 = (f32[48,2]{0,1:T(2,128)S(1)}, f32[48,2]{0,1:T(2,128)}, u32[]{:S(2)}) copy-start(f32[48,2]{0,1:T(2,128)} %param.29) | copy-start | bytes 1156
  357.3 12.7 %all-to-all-start.2 = ((bf16[4,1,48,2048]{3,2,1,0:T(8,128)(2,1)}), bf16[4,1,48,2048]{3,2,1,0:T(8,128)(2,1)S(1)}, u32[]{:S(2)}, u32[]{:S(2)}) async-start(bf16[4,1,48,2048]{3,2,1,0:T(8,128)(2,1)} %bitcast.96), calls=%async_computation.3 | async-start | bytes 1572864 | tf_op jit(solution)/shard_map/all_to_all | solution.py:158
Sparse Core Ops, SparseCore 0:
  8.9 84.8 all-gather.2
  199.4 63.4 all-gather.4
  288.9 68.3 reduce-scatter.1
where the time goes:
time: 382 us; the launch traced here: 380 us
  waiting for transfers between devices  148 us (39%)
  blocking collectives  133 us (35%)
  matrix products  35.5 us (9%)
  other arithmetic  26.7 us (7%)
  local copies, waits for them, and re-layouts  14.7 us (4%)
  between operations  13.4 us (4%)
  starting transfers between devices  8.62 us (2%)
    all_to_all x1, blocking collectives, on_device(): lax.all_to_all(outgoing.reshape(seq_devices, local_experts, capacity, mod...  96.4 us
    reduce_scatter x1, waiting for transfers between devices, on_device(): lax.psum_scatter(partials.astype(jnp.bfloat16), 'tp', scatter_dimension=0...  68.5 us
    all_gather x1, waiting for transfers between devices, on_device(): row_piece = lax.all_gather(arrived, 'tp', axis=0, tiled=True)  63.5 us
    another operation x2, other arithmetic  14.1 us
    all_gather x1, blocking collectives, on_device(): key_piece = lax.all_gather(keys, 'sp', axis=0, tiled=True)  13.4 us
    all_gather x1, blocking collectives, on_device(): value_piece = lax.all_gather(values, 'sp', axis=0, tiled=True)  12.4 us
    all_gather x1, blocking collectives, on_device(): bias_piece = lax.all_gather(key_bias, 'sp', axis=0, tiled=True)  11 us
    dot_general x1, matrix products, expert_partial(): jnp.dot(row_block, gate_matrix, preferred_element_type=jnp.float32)  9.96 us
  transfers between devices with their start and end apart: 5, of which 4 were waited for; matrix products, arithmetic and copies ran while one was open for 10% of the time, Pallas kernels for 0%

commit v1 on v0

--- a/solution.py
+++ b/solution.py
@@ -144,7 +144,23 @@
         concat_axis=0,
         tiled=True,
     )
-    row_piece = lax.all_gather(arrived, "tp", axis=0, tiled=True)
+
+    def _serve_positions(local):
+        amount_of = lax.axis_size("tp")
+        made = [local]
+        u = 1
+        while u < amount_of:
+            built = lax.ppermute(
+                made[u - 1], "tp", [(ix, (ix - 1) % amount_of) for ix in range(amount_of)]
+            )
+            made.append(built)
+            u += 1
+        t1 = jnp.concatenate(made, axis=0)
+        long_array = lax.axis_index("tp")
+        base_arr = jnp.roll(t1, long_array * local.shape[0], axis=0)
+        return base_arr
+
+    row_piece = _serve_positions(arrived)
     count_rows = row_piece.shape[0]
     partials = jnp.stack(
         [

time: 382 us -> 431 us (1.13)
  local copies, waits for them, and re-layouts: 14.7 us -> 39.4 us
  starting transfers between devices: 8.62 us -> 31.4 us
  loops' own time: 0.31 us -> 8.55 us
    all_gather x1 -> x0, waiting for transfers between devices: 63.5 us -> none  [on_device(): row_piece = lax.all_gather(arrived, 'tp', axis=0, tiled=True)]
    ppermute x0 -> x7, waiting for transfers between devices: none -> 58.3 us  [_serve_positions(): lax.ppermute(made[u - 1], 'tp', [(ix, (ix - 1) % amount_of) for ix in ran...]
    ppermute x0 -> x7, starting transfers between devices: none -> 22.9 us  [_serve_positions(): lax.ppermute(made[u - 1], 'tp', [(ix, (ix - 1) % amount_of) for ix in ran...]
    unnamed x21 -> x40, local copies, waits for them, and re-layouts: 4.15 us -> 24.4 us
    another operation x1, loops' own time: 0.2 us -> 8.44 us  [on_device(): lax.fori_loop(0, key_piece.shape[0] // rows_own, visit, empty_state)]
  transfers between devices with their start and end apart: 5 -> 11, of which waited for: 4 -> 10; matrix products, arithmetic and copies ran while one was open for 10% -> 11% of each run, Pallas kernels for 0% -> 0%
where the time goes in v1:
time: 431 us; the launch traced here: 430 us
  waiting for transfers between devices  145 us (34%)
  blocking collectives  133 us (31%)
  local copies, waits for them, and re-layouts  39.4 us (9%)
  matrix products  32.4 us (8%)
  starting transfers between devices  31.4 us (7%)
  other arithmetic  26.7 us (6%)
  between operations  14 us (3%)
  loops' own time  8.55 us (2%)
    all_to_all x1, blocking collectives, on_device(): lax.all_to_all(outgoing.reshape(seq_devices, local_experts, capacity, mod...  96.2 us
    reduce_scatter x1, waiting for transfers between devices, on_device(): lax.psum_scatter(partials.astype(jnp.bfloat16), 'tp', scatter_dimension=0...  70.2 us
    ppermute x7, waiting for transfers between devices, _serve_positions(): lax.ppermute(made[u - 1], 'tp', [(ix, (ix - 1) % amount_of) for ix in ran...  58.3 us
    unnamed x40, local copies, waits for them, and re-layouts  24.4 us
    ppermute x7, starting transfers between devices, _serve_positions(): lax.ppermute(made[u - 1], 'tp', [(ix, (ix - 1) % amount_of) for ix in ran...  22.9 us
    another operation x2, other arithmetic  14.1 us
    all_gather x1, blocking collectives, on_device(): key_piece = lax.all_gather(keys, 'sp', axis=0, tiled=True)  13.4 us
    all_gather x1, blocking collectives, on_device(): value_piece = lax.all_gather(values, 'sp', axis=0, tiled=True)  12.4 us
  transfers between devices with their start and end apart: 11, of which 10 were waited for; matrix products, arithmetic and copies ran while one was open for 11% of the time, Pallas kernels for 0%

profile of v1, /device:TPU:0, one launch (start us, length us, event | category | flops | bytes accessed | tf_op | source)
XLA Modules:
  0.0 430.1 jit_solution(11437114893456932746)
XLA Ops:
  11.2 11.0 %all_gather.14 = bf16[1536,4]{0,1:T(4,128)(2,1)} all-gather(bf16[384,4]{0,1:T(4,128)(2,1)} %param.20), channel_id=1, replica_groups=mesh['sp'=4,'tp'=8] {'sp'}, dimensions={0}, use_global_device_ids=true | all-gather | bytes 15360 | tf_op jit(solution)/shard_map/all_gather | solution.py:92
  22.2 12.4 %all_gather.12 = bf16[1536,256]{0,1:T(8,128)(2,1)} all-gather(bf16[384,256]{0,1:T(8,128)(2,1)S(1)} %copy.81), channel_id=1, replica_groups=mesh['sp'=4,'tp'=8] {'sp'}, dimensions={0}, use_global_device_ids=true | all-gather | bytes 983040 | tf_op jit(solution)/shard_map/all_gather | solution.py:91
  34.5 13.4 %all_gather.13 = bf16[1536,256]{0,1:T(8,128)(2,1)} all-gather(bf16[384,256]{0,1:T(8,128)(2,1)S(1)} %copy.82), channel_id=1, replica_groups=mesh['sp'=4,'tp'=8] {'sp'}, dimensions={0}, use_global_device_ids=true | all-gather | bytes 983040 | tf_op jit(solution)/shard_map/all_gather | solution.py:90
  49.8 36.4 %while.17 = (s32[]{:T(128)}, f32[4,384,256]{1,2,0:T(8,128)}, f32[4,4,384]{2,1,0:T(4,128)}, s32[]{:T(128)}, bf16[1536,256]{0,1:T(8,128)(2,1)}, /*index=5*/bf16[15...) while((s32[]{:T(128)}, f32[4,384,256]{1,2,0:T(8,128)}, ...), condition=%wide.region_6.7_spmd.clone.clone, body=%wide.region_0.6_spmd.clone.clone.sunk | while | flops 246117120 | bytes 38572464 | solution.py:114
  49.8 28.0 %conditional.4 = ((f32[4,384,256]{1,2,0:T(8,128)}, f32[4,4,384]{2,1,0:T(4,128)})) conditional(s32[]{:T(128)} %convert_element_type.76, (f32[4,384,256]{1,2,0:T(8,128)}, f32[4,4,384]{2,1,0:T(4,128)}) %tuple.53, (s32[]{:T(128)}, bf16[1536,256]{0,1:T(8,128)(2,1)}, s32[]{:T(128)}, bf16[1536,256]{0,1:T(8,128)(2,1)}, bf16[384,4,64]{0,2,1:T(8,128)(2,1)}, ...), branch_computations={%region_1.0_spmd, %region_2.5_spmd} | conditional | flops 246117120 | bytes 38570716 | solution.py:112
  51.7 4.3 fusion.15
  56.0 14.0 %fusion.2 = f32[4,384,3,128]{1,2,3,0:T(4,128)S(1)} fusion(f32[4,384,3,128]{1,3,2,0:T(8,128)S(1)} %bitcast.90), kind=kOutput, calls=%fused_computation.5 | output fusion | flops 74907648 | bytes 4718592 | tf_op jit(solution)/shard_map/reduce-window
  72.3 3.6 fusion.8
  91.6 4.8 %all-to-all-start = ((bf16[8,48,256]{2,1,0:T(8,128)(2,1)}), bf16[8,48,256]{2,1,0:T(8,128)(2,1)S(1)}, u32[]{:S(2)}, u32[]{:S(2)}) async-start(bf16[8,48,256]{2,1,0:T(8,128)(2,1)} %multiply_convert_fusion.2), calls=%async_computation | async-start | bytes 393216 | tf_op jit(solution)/shard_map/all_to_all | solution.py:126
  97.8 6.8 %all-to-all-done = bf16[8,48,256]{2,1,0:T(8,128)(2,1)S(1)} async-done(((bf16[8,48,256]{2,1,0:T(8,128)(2,1)}), bf16[8,48,256]{2,1,0:T(8,128)(2,1)S(1)}, u32[]{:S(2)}, u32[]{:S(2)}) %all-to-all-start) | async-done | bytes 196640 | tf_op jit(solution)/shard_map/all_to_all | solution.py:126
  104.7 5.1 %multiply_reduce_fusion.1 = (f32[48]{0:T(128)S(1)}, f32[48,2048]{1,0:T(8,128)S(1)}) fusion(bf16[48,2048]{1,0:T(8,128)(2,1)S(1)} %bitcast.98, bf16[2048,2048]{1,0:T(8,128)(2,1)} %all-gather.2.cloned.1.call-done, bf16[48,2048]{1,0:T(8,128)(2,1)S(1)} %copy-done.3), kind=kOutput, calls=%fused_computation.55 | convolution fusion | flops 403242944 | bytes 9175232 | tf_op jit(solution)/shard_map/dot_general | solution.py:127
  111.2 96.2 %all_to_all.26 = bf16[4,1,48,2048]{3,2,1,0:T(8,128)(2,1)S(1)} all-to-all(bf16[4,1,48,2048]{3,2,1,0:T(8,128)(2,1)S(1)} %broadcast_select_fusion), channel_id=1, replica_groups=mesh['sp'=4,'tp'=8] {'sp'}, dimensions={0} | all-to-all | bytes 1572864 | tf_op jit(solution)/shard_map/all_to_all | solution.py:140
  208.0 9.5 %collective-permute-done = bf16[4,1,48,2048]{3,2,1,0:T(8,128)(2,1)S(1)} collective-permute-done((bf16[4,1,48,2048]{3,2,1,0:T(8,128)(2,1)S(1)}, bf16[4,1,48,2048]{3,2,1,0:T(8,128)(2,1)S(1)}, u32[]{:S(2)}, u32[]{:S(2)}) %collective-permute-start) | collective-permute-done | bytes 786464 | tf_op jit(solution)/shard_map/ppermute | solution.py:153
  217.5 3.7 collective-permute-start.1
  221.2 9.5 %collective-permute-done.1 = bf16[4,1,48,2048]{3,2,1,0:T(8,128)(2,1)S(1)} collective-permute-done((bf16[4,1,48,2048]{3,2,1,0:T(8,128)(2,1)S(1)}, bf16[4,1,48,2048]{3,2,1,0:T(8,128)(2,1)S(1)}, u32[]{:S(2)}, u32[]{:S(2)}) %collective-permute-start.1) | collective-permute-done | bytes 786464 | tf_op jit(solution)/shard_map/ppermute | solution.py:153
  230.7 3.7 collective-permute-start.2
  234.4 9.5 %collective-permute-done.2 = bf16[4,1,48,2048]{3,2,1,0:T(8,128)(2,1)S(1)} collective-permute-done((bf16[4,1,48,2048]{3,2,1,0:T(8,128)(2,1)S(1)}, bf16[4,1,48,2048]{3,2,1,0:T(8,128)(2,1)S(1)}, u32[]{:S(2)}, u32[]{:S(2)}) %collective-permute-start.2) | collective-permute-done | bytes 786464 | tf_op jit(solution)/shard_map/ppermute | solution.py:153
  244.0 3.7 collective-permute-start.3
  247.7 9.5 %collective-permute-done.3 = bf16[4,1,48,2048]{3,2,1,0:T(8,128)(2,1)S(1)} collective-permute-done((bf16[4,1,48,2048]{3,2,1,0:T(8,128)(2,1)S(1)}, bf16[4,1,48,2048]{3,2,1,0:T(8,128)(2,1)S(1)}, u32[]{:S(2)}, u32[]{:S(2)}) %collective-permute-start.3) | collective-permute-done | bytes 786464 | tf_op jit(solution)/shard_map/ppermute | solution.py:153
  258.0 3.7 collective-permute-start.4
  261.7 9.5 %collective-permute-done.4 = bf16[4,1,48,2048]{3,2,1,0:T(8,128)(2,1)} collective-permute-done((bf16[4,1,48,2048]{3,2,1,0:T(8,128)(2,1)S(1)}, bf16[4,1,48,2048]{3,2,1,0:T(8,128)(2,1)}, u32[]{:S(2)}, u32[]{:S(2)}) %collective-permute-start.4) | collective-permute-done | bytes 786464 | tf_op jit(solution)/shard_map/ppermute | solution.py:153
  271.3 3.8 collective-permute-start.5
  277.9 7.0 %collective-permute-done.5 = bf16[4,1,48,2048]{3,2,1,0:T(8,128)(2,1)} collective-permute-done((bf16[4,1,48,2048]{3,2,1,0:T(8,128)(2,1)}, bf16[4,1,48,2048]{3,2,1,0:T(8,128)(2,1)}, u32[]{:S(2)}, u32[]{:S(2)}) %collective-permute-start.5) | collective-permute-done | bytes 786464 | tf_op jit(solution)/shard_map/ppermute | solution.py:153
  284.9 3.7 collective-permute-start.6
  294.7 3.7 collective-permute-done.6
  309.5 3.5 constant_dynamic-slice_fusion.2
  313.3 6.7 %fusion.21 = f32[1536,896]{1,0:T(8,128)S(1)} fusion(bf16[1536,2048]{1,0:T(8,128)(2,1)S(1)} %bitcast.94, bf16[1,2048,896]{2,1,0:T(8,128)(2,1)S(1)} %copy-done.8), kind=kOutput, calls=%fused_computation.39 | convolution fusion | flops 5637144576 | bytes 15466496 | tf_op jit(solution)/shard_map/dot_general | solution.py:14
  320.1 7.3 %multiply_convert_fusion = bf16[1536,896]{1,0:T(8,128)(2,1)S(1)} fusion(f32[1536,896]{1,0:T(8,128)S(1)} %fusion.21, bf16[1536,2048]{1,0:T(8,128)(2,1)S(1)} %bitcast.95, bf16[1,2048,896]{2,1,0:T(8,128)(2,1)S(1)} %copy-done.9), kind=kOutput, calls=%fused_computation.35 | convolution fusion | flops 5645402112 | bytes 18219008 | tf_op jit(solution)/shard_map/dot_general | solution.py:15
  327.4 8.7 %convert_bitcast_fusion.1 = bf16[32,1,48,2048]{3,2,0,1:T(8,128)(2,1)} fusion(bf16[32,48,896]{2,1,0:T(8,128)(2,1)S(1)} %bitcast.105, bf16[1,896,2048]{2,1,0:T(8,128)(2,1)S(1)} %copy-done.10), kind=kOutput, calls=%fused_computation.34 | convolution fusion | flops 5640290304 | bytes 12713984 | tf_op jit(solution)/shard_map/dot_general | solution.py:17
  336.1 70.2 %reduce-scatter.2.cloned.1.call-done = bf16[4,1,48,2048]{3,2,0,1:T(8,128)(2,1)} async-done(((bf16[32,1,48,2048]{3,2,0,1:T(8,128)(2,1)}), bf16[4,1,48,2048]{3,2,0,1:T(8,128)(2,1)}) %reduce-scatter.2.cloned.1.call-update) | async-done | bytes 786448 | tf_op jit(solution)/shard_map/reduce_scatter | solution.py:173
  406.3 3.6 all-to-all-start.2
  410.4 8.6 %all-to-all-done.2 = bf16[4,1,48,2048]{3,2,1,0:T(8,128)(2,1)S(1)} async-done(((bf16[4,1,48,2048]{3,2,1,0:T(8,128)(2,1)}), bf16[4,1,48,2048]{3,2,1,0:T(8,128)(2,1)S(1)}, u32[]{:S(2)}, u32[]{:S(2)}) %all-to-all-start.2) | async-done | bytes 786464 | tf_op jit(solution)/shard_map/all_to_all | solution.py:174
  (112 shorter events, 46.7 us)
Async XLA Ops:
  6.5 98.1 %all-gather.2.cloned.1.call-start = ((), (), s32[]{:S(2)}) async-start(), calls=%async_computation.4 | async-start | bytes 9437184 | tf_op jit(solution)/shard_map/all_gather | solution.py:129
  70.6 1.7 copy-start
  86.2 4.5 %copy-start.6 = (f32[4,64]{1,0:T(4,128)S(1)}, f32[4,64]{1,0:T(4,128)}, u32[]{:S(2)}) copy-start(f32[4,64]{1,0:T(4,128)} %param.21) | copy-start | bytes 3076
  86.2 10.2 %copy-start.5 = (s32[48,2]{0,1:T(2,128)S(1)}, s32[48,2]{0,1:T(2,128)}, u32[]{:S(2)}) copy-start(s32[48,2]{0,1:T(2,128)} %param.28) | copy-start | bytes 1156
  87.7 16.9 %copy-start.3 = (bf16[48,2048]{1,0:T(8,128)(2,1)S(1)}, bf16[48,2048]{1,0:T(8,128)(2,1)}, u32[]{:S(2)}) copy-start(bf16[48,2048]{1,0:T(8,128)(2,1)} %param.23) | copy-start | bytes 589828
  91.6 13.1 %all-to-all-start = ((bf16[8,48,256]{2,1,0:T(8,128)(2,1)}), bf16[8,48,256]{2,1,0:T(8,128)(2,1)S(1)}, u32[]{:S(2)}, u32[]{:S(2)}) async-start(bf16[8,48,256]{2,1,0:T(8,128)(2,1)} %multiply_convert_fusion.2), calls=%async_computation | async-start | bytes 393216 | tf_op jit(solution)/shard_map/all_to_all | solution.py:126
  96.3 310.0 %reduce-scatter.2.cloned.1.call-start = ((), (), s32[]{:S(2)}) async-start(), calls=%async_computation.5 | async-start | bytes 7077888 | tf_op jit(solution)/shard_map/reduce_scatter | solution.py:173
  104.7 5.1 %copy-start.4 = (f32[2048]{0:T(1024)S(1)}, f32[2048]{0:T(1024)}, u32[]{:S(2)}) copy-start(f32[2048]{0:T(1024)} %param.24) | copy-start | bytes 24580
  207.4 10.1 %collective-permute-start = (bf16[4,1,48,2048]{3,2,1,0:T(8,128)(2,1)S(1)}, bf16[4,1,48,2048]{3,2,1,0:T(8,128)(2,1)S(1)}, u32[]{:S(2)}, u32[]{:S(2)}) collective-permute-start(bf16[4,1,48,2048]{3,2,1,0:T(8,128)(2,1)S(1)} %all_to_all.26), channel_id=1, source_target_pairs={{0,7},{1,0},{2,1},{3,2},{4,3},{5,4},{6,5},{7,6},{8,15},{9,8},{10,9... | collective-permute-start | bytes 2359304 | tf_op jit(solution)/shard_map/ppermute | solution.py:153
  217.5 13.2 %collective-permute-start.1 = (bf16[4,1,48,2048]{3,2,1,0:T(8,128)(2,1)S(1)}, bf16[4,1,48,2048]{3,2,1,0:T(8,128)(2,1)S(1)}, u32[]{:S(2)}, u32[]{:S(2)}) collective-permute-start(bf16[4,1,48,2048]{3,2,1,0:T(8,128)(2,1)S(1)} %collective-permute-done), channel_id=1, source_target_pairs={{0,7},{1,0},{2,1},{3,2},{4,3},{5,4},{6,5},{7,6},{8,15},{9,8},{10,9... | collective-permute-start | bytes 2359304 | tf_op jit(solution)/shard_map/ppermute | solution.py:153
  230.7 13.2 %collective-permute-start.2 = (bf16[4,1,48,2048]{3,2,1,0:T(8,128)(2,1)S(1)}, bf16[4,1,48,2048]{3,2,1,0:T(8,128)(2,1)S(1)}, u32[]{:S(2)}, u32[]{:S(2)}) collective-permute-start(bf16[4,1,48,2048]{3,2,1,0:T(8,128)(2,1)S(1)} %collective-permute-done.1), channel_id=1, source_target_pairs={{0,7},{1,0},{2,1},{3,2},{4,3},{5,4},{6,5},{7,6},{8,15},{9,8},{10,9... | collective-permute-start | bytes 2359304 | tf_op jit(solution)/shard_map/ppermute | solution.py:153
  244.0 13.2 %collective-permute-start.3 = (bf16[4,1,48,2048]{3,2,1,0:T(8,128)(2,1)S(1)}, bf16[4,1,48,2048]{3,2,1,0:T(8,128)(2,1)S(1)}, u32[]{:S(2)}, u32[]{:S(2)}) collective-permute-start(bf16[4,1,48,2048]{3,2,1,0:T(8,128)(2,1)S(1)} %collective-permute-done.2), channel_id=1, source_target_pairs={{0,7},{1,0},{2,1},{3,2},{4,3},{5,4},{6,5},{7,6},{8,15},{9,8},{10,9... | collective-permute-start | bytes 2359304 | tf_op jit(solution)/shard_map/ppermute | solution.py:153
  257.2 0.9 copy-start.1
  258.0 13.2 %collective-permute-start.4 = (bf16[4,1,48,2048]{3,2,1,0:T(8,128)(2,1)S(1)}, bf16[4,1,48,2048]{3,2,1,0:T(8,128)(2,1)}, u32[]{:S(2)}, u32[]{:S(2)}) collective-permute-start(bf16[4,1,48,2048]{3,2,1,0:T(8,128)(2,1)S(1)} %collective-permute-done.3), channel_id=1, source_target_pairs={{0,7},{1,0},{2,1},{3,2},{4,3},{5,4},{6,5},{7,6},{8,15},{9,8},{10,9... | collective-permute-start | bytes 2359304 | tf_op jit(solution)/shard_map/ppermute | solution.py:153
  271.3 13.6 %collective-permute-start.5 = (bf16[4,1,48,2048]{3,2,1,0:T(8,128)(2,1)}, bf16[4,1,48,2048]{3,2,1,0:T(8,128)(2,1)}, u32[]{:S(2)}, u32[]{:S(2)}) collective-permute-start(bf16[4,1,48,2048]{3,2,1,0:T(8,128)(2,1)} %collective-permute-done.4), channel_id=1, source_target_pairs={{0,7},{1,0},{2,1},{3,2},{4,3},{5,4},{6,5},{7,6},{8,15},{9,8},{10,9... | collective-permute-start | bytes 2359304 | tf_op jit(solution)/shard_map/ppermute | solution.py:153
  275.1 14.5 %copy-start.2 = (bf16[4,1,48,2048]{3,2,1,0:T(8,128)(2,1)S(1)}, bf16[4,1,48,2048]{3,2,1,0:T(8,128)(2,1)}, u32[]{:S(2)}) copy-start(bf16[4,1,48,2048]{3,2,1,0:T(8,128)(2,1)} %copy-done.1) | copy-start | bytes 2359300
  284.9 13.5 %collective-permute-start.6 = (bf16[4,1,48,2048]{3,2,1,0:T(8,128)(2,1)}, bf16[4,1,48,2048]{3,2,1,0:T(8,128)(2,1)S(1)}, u32[]{:S(2)}, u32[]{:S(2)}) collective-permute-start(bf16[4,1,48,2048]{3,2,1,0:T(8,128)(2,1)} %collective-permute-done.5), channel_id=1, source_target_pairs={{0,7},{1,0},{2,1},{3,2},{4,3},{5,4},{6,5},{7,6},{8,15},{9,8},{10,9... | collective-permute-start | bytes 2359304 | tf_op jit(solution)/shard_map/ppermute | solution.py:153
  309.5 3.9 copy-start.8
  313.3 6.7 %copy-start.9 = (bf16[1,2048,896]{2,1,0:T(8,128)(2,1)S(1)}, bf16[1,2048,896]{2,1,0:T(8,128)(2,1)}, u32[]{:S(2)}) copy-start(bf16[1,2048,896]{2,1,0:T(8,128)(2,1)} %param.26) | copy-start | bytes 11010052
  320.1 7.3 %copy-start.10 = (bf16[1,896,2048]{2,1,0:T(8,128)(2,1)S(1)}, bf16[1,896,2048]{2,1,0:T(8,128)(2,1)}, u32[]{:S(2)}) copy-start(bf16[1,896,2048]{2,1,0:T(8,128)(2,1)} %param.27) | copy-start | bytes 11010052
  336.1 74.2 %copy-start.7 = (f32[48,2]{0,1:T(2,128)S(1)}, f32[48,2]{0,1:T(2,128)}, u32[]{:S(2)}) copy-start(f32[48,2]{0,1:T(2,128)} %param.29) | copy-start | bytes 1156
  406.3 12.7 %all-to-all-start.2 = ((bf16[4,1,48,2048]{3,2,1,0:T(8,128)(2,1)}), bf16[4,1,48,2048]{3,2,1,0:T(8,128)(2,1)S(1)}, u32[]{:S(2)}, u32[]{:S(2)}) async-start(bf16[4,1,48,2048]{3,2,1,0:T(8,128)(2,1)} %bitcast.100), calls=%async_computation.3 | async-start | bytes 1572864 | tf_op jit(solution)/shard_map/all_to_all | solution.py:174
Sparse Core Ops, SparseCore 0:
  8.9 84.7 all-gather.1
  336.2 70.0 reduce-scatter.1
